TPU v7x, 32 devices: a whole 2x2x4 slice. The times are simulated.
32 devices in a mesh: sp: 8 (over z, y), tp: 4 (over x, core).
Axes of the slice: x: 2, y: 2, z: 4, core: 2. Of those that a mesh axis runs over, the one named last changes fastest.
Arguments:
- queries: bfloat16 [4096, 1024], P('sp', 'tp'), may hold values from -200 to 200
- keys: bfloat16 [4096, 1024], P('sp', 'tp'), may hold values from -6 to 6
- values: bfloat16 [4096, 1024], P('sp', 'tp'), may hold values from -24 to 24
- cum_gate: float32 [4096, 8], P('sp', 'tp'), may hold values from -414 to 0, as said below
- residual: bfloat16 [4096, 2048], P(('sp', 'tp')), may hold values from -1.5 to 1.5
- w_out: bfloat16 [1024, 2048], replicated, may hold values from -0.1875 to 0.1875
- gain: float32 [2048], replicated, may hold values from 0.1 to 1.9
- w_up: bfloat16 [2048, 8192], P('sp', 'tp'), may hold values from -0.125 to 0.125
- w_down: bfloat16 [8192, 2048], P('tp', 'sp'), may hold values from -0.0625 to 0.0625
Outputs:
- output: bfloat16 [4096, 2048], P(('sp', 'tp'))
Inputs may be any that keep to these rules, and one draw needn't show every extreme that they name: Within each head, cum_gate never rises from one position to the next.
All inputs are finite; a program needn't handle non-finite values.
Results may differ from a plain program's by a relative error of at most 0.022.
Values may be sent and summed in bfloat16 or wider, within the bound.
A program may use at most 128 MiB of HBM per device.

v0:
```python
import math
import jax
import jax.numpy as jnp
from jax import lax
from jax.sharding import PartitionSpec as P


def per_device(queries, keys, values, cum_gate, residual, w_out, gain, w_up, w_down):
    tok_rows, width = queries.shape
    heads_here = cum_gate.shape[1]
    head_size = width // heads_here
    score_scale = head_size ** (-0.5)
    row_offset = lax.axis_index("sp") * tok_rows
    query_heads = queries.reshape(tok_rows, heads_here, head_size)
    query_pos = row_offset + jnp.arange(tok_rows, dtype=jnp.int32)
    all_gates = lax.all_gather(cum_gate, "sp", axis=0, tiled=True)
    initial = (
        jnp.full((tok_rows, heads_here), -1e30, jnp.float32),
        jnp.zeros((tok_rows, heads_here), jnp.float32),
        jnp.zeros((tok_rows, heads_here, head_size), jnp.float32),
    )
    carried = initial
    key_rows = lax.all_gather(keys, "sp", axis=0, tiled=True)
    value_rows = lax.all_gather(values, "sp", axis=0, tiled=True)
    row_count = key_rows.shape[0]
    span_rows = math.gcd(row_count, 2048)
    block_count = row_count // span_rows
    key_blocks = key_rows.reshape(block_count, span_rows, heads_here, head_size)
    value_blocks = value_rows.reshape(block_count, span_rows, heads_here, head_size)
    first_pos = jnp.arange(block_count, dtype=jnp.int32) * span_rows

    def absorb_block(running, packed):
        running_max, running_sum, accumulated = running
        key_blk, value_blk, block_start = packed
        gate_blk = lax.dynamic_slice_in_dim(all_gates, block_start, span_rows, 0)
        scores = jnp.einsum(
            "qhd,khd->qhk", query_heads, key_blk, preferred_element_type=jnp.float32
        )
        scores = scores * score_scale + cum_gate[:, :, None] - gate_blk.T[None, :, :]
        key_pos = block_start + jnp.arange(span_rows, dtype=jnp.int32)
        scores = jnp.where(key_pos[None, None, :] <= query_pos[:, None, None], scores, -1e30)
        new_max = jnp.maximum(running_max, jnp.max(scores, axis=-1))
        rescale = jnp.exp(running_max - new_max)
        weights = jnp.exp(scores - new_max[:, :, None])
        running_sum = running_sum * rescale + jnp.sum(weights, axis=-1)
        product = jnp.einsum(
            "qhk,khd->qhd",
            weights.astype(jnp.bfloat16),
            value_blk,
            preferred_element_type=jnp.float32,
        )
        accumulated = accumulated * rescale[:, :, None] + product
        return ((new_max, running_sum, accumulated), None)

    carried, _ = lax.scan(absorb_block, carried, (key_blocks, value_blocks, first_pos))
    running_max, running_sum, accumulated = carried
    attended = (accumulated / running_sum[:, :, None]).reshape(tok_rows, width).astype(jnp.bfloat16)
    mine = lax.all_to_all(attended, "tp", split_axis=0, concat_axis=1, tiled=True)
    projected = jnp.dot(mine, w_out, preferred_element_type=jnp.float32)
    residual_sum = residual.astype(jnp.float32) + projected
    mean_square = jnp.mean(residual_sum * residual_sum, axis=-1, keepdims=True)
    normed = (residual_sum * lax.rsqrt(mean_square + 1e-06) * gain).astype(jnp.bfloat16)
    normed_all = lax.all_gather(normed, "tp", axis=0, tiled=True)
    up_proj = jnp.dot(
        normed_all,
        lax.all_gather(w_up, "sp", axis=0, tiled=True),
        preferred_element_type=jnp.float32,
    )
    hidden = jnp.square(jax.nn.relu(up_proj)).astype(jnp.bfloat16)
    down_whole = lax.all_gather(w_down, "sp", axis=1, tiled=True)
    rounded = jnp.dot(hidden, down_whole, preferred_element_type=jnp.float32).astype(jnp.bfloat16)
    branch_out = lax.psum_scatter(
        lax.optimization_barrier(rounded).astype(jnp.float32).astype(jnp.bfloat16),
        "tp",
        scatter_dimension=0,
        tiled=True,
    ).astype(jnp.float32)
    return (residual_sum + branch_out).astype(jnp.bfloat16)


def solution(mesh):
    return jax.shard_map(
        per_device,
        mesh=mesh,
        in_specs=(
            P("sp", "tp"),
            P("sp", "tp"),
            P("sp", "tp"),
            P("sp", "tp"),
            P(("sp", "tp"), None),
            P(),
            P(),
            P("sp", "tp"),
            P("tp", "sp"),
        ),
        out_specs=P(("sp", "tp"), None),
        check_vma=False,
    )
```

profile of v0, /device:TPU:0, one launch (start us, length us, event | category | flops | bytes accessed | tf_op | source)
XLA Modules:
  0.0 501.9 jit_solution(15590965651173478988)
XLA Ops:
  6.5 0.7 all-gather.6.cloned.1.call-update
  7.3 0.7 all-gather.8.cloned.1.call-update
  8.1 1.1 copy.17
  9.4 32.7 %all_gather.19 = f32[4096,2]{0,1:T(2,128)S(1)} all-gather(f32[512,2]{0,1:T(2,128)} %param.14), channel_id=1, replica_groups=mesh['sp'=8,'tp'=4] {'sp'}, dimensions={0}, use_global_device_ids=true | all-gather | bytes 36864 | tf_op jit(solution)/shard_map/all_gather | solution.py:16
  42.0 19.4 %all-gather.6.cloned.1.call-done = bf16[4096,256]{1,0:T(8,128)(2,1)} async-done(((bf16[512,256]{1,0:T(8,128)(2,1)}), bf16[4096,256]{1,0:T(8,128)(2,1)}) %all-gather.6.cloned.1.call-update) | async-done | bytes 2097168 | tf_op jit(solution)/shard_map/all_gather | solution.py:23
  61.4 4.0 reshape.62
  65.4 45.8 %all-gather.8.cloned.1.call-done = bf16[4096,256]{1,0:T(8,128)(2,1)} async-done(((bf16[512,256]{1,0:T(8,128)(2,1)}), bf16[4096,256]{1,0:T(8,128)(2,1)}) %all-gather.8.cloned.1.call-update) | async-done | bytes 2097168 | tf_op jit(solution)/shard_map/all_gather | solution.py:24
  111.2 4.0 reshape.64
  115.2 45.9 %while.15 = (s32[]{:T(128)}, f32[512,2]{0,1:T(2,128)S(1)}, f32[512,2]{0,1:T(2,128)S(1)}, f32[512,2,128]{0,2,1:T(8,128)}, s32[2]{0:T(128)S(1)}, /*index=5*/bf16[2...) while((s32[]{:T(128)}, f32[512,2]{0,1:T(2,128)S(1)}, ...), condition=%wide.region_3.4_spmd.clone, body=%wide.region_0.3_spmd.clone.sunk | while | flops 1110842880 | bytes 39239884 | solution.py:55
  115.2 0.6 dynamic_slice.26
  118.1 0.8 broadcast_compare_fusion.2
  118.9 2.7 constant_dynamic-slice_fusion.3
  121.6 4.6 fusion.40
  126.2 4.8 fusion.42
  131.0 0.8 copy.34
  131.8 6.2 %fusion.44 = f32[512,2,128]{0,2,1:T(8,128)} fusion(f32[2,2048,512]{2,1,0:T(8,128)} %get-tuple-element.231, f32[512,2]{0,1:T(2,128)S(1)} %fusion.41, f32[2,2048]{1,0:T(2,128)S(1)} %dynamic-slice_bitcast_fusion.2, f32[512,2]{0,1:T(2,128)S(1)} %get-tuple-element.270, pred[512,2048]{0,1:T(8,128)(4,1)S(1)} %broadcast_compare_fusion.2, ...), kind=kOutput, calls=%fused_computation.12.clone.1 | convolution fusion | flops 549847040 | bytes 11563009 | tf_op jit(solution)/shard_map/while/body/eval_jaxpr/qhk,khd->qhd/dot_general | solution.py:46
  141.0 0.8 broadcast_compare_fusion.2
  141.8 2.7 constant_dynamic-slice_fusion.3
  144.5 4.6 fusion.40
  149.1 4.8 fusion.42
  153.9 0.8 copy.34
  154.7 6.4 %fusion.44 = f32[512,2,128]{0,2,1:T(8,128)} fusion(f32[2,2048,512]{2,1,0:T(8,128)} %get-tuple-element.231, f32[512,2]{0,1:T(2,128)S(1)} %fusion.41, f32[2,2048]{1,0:T(2,128)S(1)} %dynamic-slice_bitcast_fusion.2, f32[512,2]{0,1:T(2,128)S(1)} %get-tuple-element.270, pred[512,2048]{0,1:T(8,128)(4,1)S(1)} %broadcast_compare_fusion.2, ...), kind=kOutput, calls=%fused_computation.12.clone.1 | convolution fusion | flops 549847040 | bytes 11563009 | tf_op jit(solution)/shard_map/while/body/eval_jaxpr/qhk,khd->qhd/dot_general | solution.py:46
  161.1 1.1 divide_convert_fusion
  162.4 8.5 %all_to_all.16 = bf16[4,128,256]{2,1,0:T(8,128)(2,1)S(1)} all-to-all(bf16[4,128,256]{2,1,0:T(8,128)(2,1)S(1)} %copy.24), channel_id=1, replica_groups=mesh['sp'=8,'tp'=4] {'tp'}, dimensions={0} | all-to-all | bytes 524288 | tf_op jit(solution)/shard_map/all_to_all | solution.py:58
  171.1 3.1 multiply_reduce_fusion
  174.3 0.9 multiply_convert_fusion.1
  176.7 19.0 %all-gather.10.cloned.1.call-done = bf16[512,2048]{1,0:T(8,128)(2,1)} async-done(((bf16[128,2048]{1,0:T(8,128)(2,1)}), bf16[512,2048]{1,0:T(8,128)(2,1)}) %all-gather.10.cloned.1.call-update) | async-done | bytes 2097168 | tf_op jit(solution)/shard_map/all_gather | solution.py:63
  195.6 126.5 %all-gather.12.cloned.1.call-done = bf16[2048,2048]{1,0:T(8,128)(2,1)} async-done(((bf16[256,2048]{1,0:T(8,128)(2,1)}), bf16[2048,2048]{1,0:T(8,128)(2,1)}) %all-gather.12.cloned.1.call-update) | async-done | bytes 8388624 | tf_op jit(solution)/shard_map/all_gather | solution.py:66
  322.1 125.0 %all-gather.14.cloned.1.call-done = bf16[2048,2048]{1,0:T(8,128)(2,1)} async-done(((bf16[2048,256]{1,0:T(8,128)(2,1)}), bf16[2048,2048]{1,0:T(8,128)(2,1)}) %all-gather.14.cloned.1.call-update) | async-done | bytes 8388624 | tf_op jit(solution)/shard_map/all_gather | solution.py:70
  447.1 16.5 %convolution_convert_fusion = bf16[512,2048]{1,0:T(8,128)(2,1)} fusion(bf16[2048,2048]{1,0:T(8,128)(2,1)} %all-gather.14.cloned.1.call-done, bf16[512,2048]{1,0:T(8,128)(2,1)} %all-gather.10.cloned.1.call-done, bf16[2048,2048]{1,0:T(8,128)(2,1)} %all-gather.12.cloned.1.call-done), kind=kOutput, calls=%fused_computation.30 | convolution fusion | flops 8594128896 | bytes 20971520 | tf_op jit(solution)/shard_map/dot_general | solution.py:71
  463.7 29.5 %reduce-scatter.2.cloned.1.call-done = bf16[128,2048]{1,0:T(8,128)(2,1)} async-done(((bf16[512,2048]{1,0:T(8,128)(2,1)}), bf16[128,2048]{1,0:T(8,128)(2,1)}) %reduce-scatter.2.cloned.1.call-update) | async-done | bytes 524304 | tf_op jit(solution)/shard_map/reduce_scatter | solution.py:72
  493.2 1.9 add_convert_fusion
  (36 shorter events, 4.0 us)
Async XLA Ops:
  6.5 108.6 %copy-start = (f32[512,2]{0,1:T(2,128)S(1)}, f32[512,2]{0,1:T(2,128)}, u32[]{:S(2)}) copy-start(f32[512,2]{0,1:T(2,128)} %param.14) | copy-start | bytes 12292
  6.5 54.9 %all-gather.6.cloned.1.call-start = ((), (), s32[]{:S(2)}) async-start(), calls=%async_computation.2 | async-start | bytes 2359296 | tf_op jit(solution)/shard_map/all_gather | solution.py:23
  7.3 103.9 %all-gather.8.cloned.1.call-start = ((), (), s32[]{:S(2)}) async-start(), calls=%async_computation.3 | async-start | bytes 2359296 | tf_op jit(solution)/shard_map/all_gather | solution.py:24
  8.0 187.6 %all-gather.10.cloned.1.call-start = ((), (), s32[]{:S(2)}) async-start(), calls=%async_computation.4 | async-start | bytes 2621440 | tf_op jit(solution)/shard_map/all_gather | solution.py:63
  161.1 13.2 %copy-start.1 = (f32[2048]{0:T(1024)S(1)}, f32[2048]{0:T(1024)}, u32[]{:S(2)}) copy-start(f32[2048]{0:T(1024)} %param.17) | copy-start | bytes 24580
  175.3 146.8 %all-gather.12.cloned.1.call-start = ((), (), s32[]{:S(2)}) async-start(), calls=%async_computation.5 | async-start | bytes 9437184 | tf_op jit(solution)/shard_map/all_gather | solution.py:66
  175.8 271.3 %all-gather.14.cloned.1.call-start = ((), (), s32[]{:S(2)}) async-start(), calls=%async_computation.6 | async-start | bytes 9437184 | tf_op jit(solution)/shard_map/all_gather | solution.py:70
  176.4 316.7 %reduce-scatter.2.cloned.1.call-start = ((), (), s32[]{:S(2)}) async-start(), calls=%async_computation.7 | async-start | bytes 2621440 | tf_op jit(solution)/shard_map/reduce_scatter | solution.py:72
Sparse Core Ops, SparseCore 0:
  9.5 51.9 all-gather.5
  63.5 47.6 all-gather.7
  175.4 20.1 all-gather.9
  197.6 124.4 all-gather.11
  324.0 123.1 all-gather.13
  463.8 29.3 reduce-scatter.1
where the time goes:
time: 502 us
  waiting for transfers between devices  368 us (73%)
  matrix products  41.4 us (8%)
  blocking collectives  41.2 us (8%)
  local copies, waits for them, and re-layouts  18 us (4%)
  other arithmetic  16.3 us (3%)
  between operations  13.6 us (3%)
    all_gather x1, waiting for transfers between devices, per_device(): lax.all_gather(w_up, 'sp', axis=0, tiled=True)  126 us
    all_gather x1, waiting for transfers between devices, per_device(): down_whole = lax.all_gather(w_down, 'sp', axis=1, tiled=True)  125 us
    all_gather x1, waiting for transfers between devices, per_device(): value_rows = lax.all_gather(values, 'sp', axis=0, tiled=True)  45.8 us
    all_gather x1, blocking collectives, per_device(): all_gates = lax.all_gather(cum_gate, 'sp', axis=0, tiled=True)  32.7 us
    reduce_scatter x1, waiting for transfers between devices, per_device(): lax.psum_scatter(lax.optimization_barrier(rounded).astype(jnp.float32).as...  29.5 us
    all_gather x1, waiting for transfers between devices, per_device(): key_rows = lax.all_gather(keys, 'sp', axis=0, tiled=True)  19.4 us
    all_gather x1, waiting for transfers between devices, per_device(): normed_all = lax.all_gather(normed, 'tp', axis=0, tiled=True)  19 us
    dot_general x1, matrix products, per_device(): jnp.dot(hidden, down_whole, preferred_element_type=jnp.float32)  16.5 us
  transfers between devices with their start and end apart: 6, of which 6 were waited for; matrix products, arithmetic and copies ran while one was open for 1% of the time, Pallas kernels for 0%

commit v1 on v0

--- a/solution.py
+++ b/solution.py
@@ -20,8 +20,9 @@
         jnp.zeros((tok_rows, heads_here, head_size), jnp.float32),
     )
     carried = initial
-    key_rows = lax.all_gather(keys, "sp", axis=0, tiled=True)
-    value_rows = lax.all_gather(values, "sp", axis=0, tiled=True)
+    y1 = jnp.concatenate([keys, values], axis=1)
+    back = jax.lax.all_gather(y1, "sp", tiled=True, axis=0)
+    key_rows, value_rows = jnp.split(back, [keys.shape[1]], 1)
     row_count = key_rows.shape[0]
     span_rows = math.gcd(row_count, 2048)
     block_count = row_count // span_rows

time: 502 us -> 483 us (0.962)
  waiting for transfers between devices: 368 us -> 343 us
    all_gather x2 -> x1, waiting for transfers between devices: 65.1 us -> 42.2 us  [per_device(): back = jax.lax.all_gather(y1, 'sp', tiled=True, axis=0)]
  transfers between devices with their start and end apart: 6 -> 5, of which waited for: 6 -> 5; matrix products, arithmetic and copies ran while one was open for 1% -> 0% of each run, Pallas kernels for 0% -> 0%
where the time goes in v1:
time: 483 us; the launch traced here: 482 us
  waiting for transfers between devices  343 us (71%)
  blocking collectives  41.8 us (9%)
  matrix products  41.4 us (9%)
  local copies, waits for them, and re-layouts  20 us (4%)
  other arithmetic  18.3 us (4%)
  between operations  13.2 us (3%)
    all_gather x1, waiting for transfers between devices, per_device(): down_whole = lax.all_gather(w_down, 'sp', axis=1, tiled=True)  127 us
    all_gather x1, waiting for transfers between devices, per_device(): lax.all_gather(w_up, 'sp', axis=0, tiled=True)  125 us
    all_gather x1, waiting for transfers between devices, per_device(): back = jax.lax.all_gather(y1, 'sp', tiled=True, axis=0)  42.2 us
    all_gather x1, blocking collectives, per_device(): all_gates = lax.all_gather(cum_gate, 'sp', axis=0, tiled=True)  33.2 us
    reduce_scatter x1, waiting for transfers between devices, per_device(): lax.psum_scatter(lax.optimization_barrier(rounded).astype(jnp.float32).as...  29.5 us
    all_gather x1, waiting for transfers between devices, per_device(): normed_all = lax.all_gather(normed, 'tp', axis=0, tiled=True)  18.8 us
    dot_general x1, matrix products, per_device(): jnp.dot(hidden, down_whole, preferred_element_type=jnp.float32)  16.5 us
    dot_general x2, matrix products, absorb_block(): jnp.einsum('qhk,khd->qhd', weights.astype(jnp.bfloat16), value_blk, prefe...  12.6 us
  transfers between devices with their start and end apart: 5, of which 5 were waited for; matrix products, arithmetic and copies ran while one was open for 0% of the time, Pallas kernels for 0%

profile of v1, /device:TPU:0, one launch (start us, length us, event | category | flops | bytes accessed | tf_op | source)
XLA Modules:
  0.0 482.3 jit_solution(15498138060287067180)
XLA Ops:
  6.5 1.9 pad_maximum_fusion
  8.5 1.1 copy.17
  9.8 33.2 %all_gather.16 = f32[4096,2]{0,1:T(2,128)S(1)} all-gather(f32[512,2]{0,1:T(2,128)} %param.14), channel_id=1, replica_groups=mesh['sp'=8,'tp'=4] {'sp'}, dimensions={0}, use_global_device_ids=true | all-gather | bytes 36864 | tf_op jit(solution)/shard_map/all_gather | solution.py:16
  43.0 42.2 %all-gather.5.cloned.1.call-done = bf16[4096,512]{1,0:T(8,128)(2,1)} async-done(((bf16[512,512]{1,0:T(8,128)(2,1)}), bf16[4096,512]{1,0:T(8,128)(2,1)}) %all-gather.5.cloned.1.call-update) | async-done | bytes 4194320 | tf_op jit(solution)/shard_map/all_gather | solution.py:24
  85.2 3.8 fusion.23
  89.0 4.0 reshape.62
  93.0 2.1 reshape.64
  95.1 46.5 %while.15 = (s32[]{:T(128)}, f32[512,2]{0,1:T(2,128)S(1)}, f32[512,2]{0,1:T(2,128)S(1)}, f32[512,2,128]{0,2,1:T(8,128)}, s32[2]{0:T(128)S(1)}, /*index=5*/bf16[2...) while((s32[]{:T(128)}, f32[512,2]{0,1:T(2,128)S(1)}, ...), condition=%wide.region_3.4_spmd.clone, body=%wide.region_0.3_spmd.clone.sunk | while | flops 1110842880 | bytes 39239884 | solution.py:56
  95.1 0.6 dynamic_slice.26
  98.3 0.8 broadcast_compare_fusion.2
  99.1 2.7 constant_dynamic-slice_fusion.3
  101.8 4.6 fusion.41
  106.4 4.8 fusion.43
  111.2 0.8 copy.34
  112.0 6.2 %fusion.45 = f32[512,2,128]{0,2,1:T(8,128)} fusion(f32[2,2048,512]{2,1,0:T(8,128)} %get-tuple-element.233, f32[512,2]{0,1:T(2,128)S(1)} %fusion.42, f32[2,2048]{1,0:T(2,128)S(1)} %dynamic-slice_bitcast_fusion.2, f32[512,2]{0,1:T(2,128)S(1)} %get-tuple-element.272, pred[512,2048]{0,1:T(8,128)(4,1)S(1)} %broadcast_compare_fusion.2, ...), kind=kOutput, calls=%fused_computation.12.clone.1 | convolution fusion | flops 549847040 | bytes 11563009 | tf_op jit(solution)/shard_map/while/body/eval_jaxpr/qhk,khd->qhd/dot_general | solution.py:47
  121.5 0.8 broadcast_compare_fusion.2
  122.3 2.7 constant_dynamic-slice_fusion.3
  125.0 4.6 fusion.41
  129.6 4.8 fusion.43
  134.4 0.8 copy.34
  135.2 6.4 %fusion.45 = f32[512,2,128]{0,2,1:T(8,128)} fusion(f32[2,2048,512]{2,1,0:T(8,128)} %get-tuple-element.233, f32[512,2]{0,1:T(2,128)S(1)} %fusion.42, f32[2,2048]{1,0:T(2,128)S(1)} %dynamic-slice_bitcast_fusion.2, f32[512,2]{0,1:T(2,128)S(1)} %get-tuple-element.272, pred[512,2048]{0,1:T(8,128)(4,1)S(1)} %broadcast_compare_fusion.2, ...), kind=kOutput, calls=%fused_computation.12.clone.1 | convolution fusion | flops 549847040 | bytes 11563009 | tf_op jit(solution)/shard_map/while/body/eval_jaxpr/qhk,khd->qhd/dot_general | solution.py:47
  141.6 1.1 divide_convert_fusion
  142.9 8.5 %all_to_all.16 = bf16[4,128,256]{2,1,0:T(8,128)(2,1)S(1)} all-to-all(bf16[4,128,256]{2,1,0:T(8,128)(2,1)S(1)} %copy.24), channel_id=1, replica_groups=mesh['sp'=8,'tp'=4] {'tp'}, dimensions={0} | all-to-all | bytes 524288 | tf_op jit(solution)/shard_map/all_to_all | solution.py:59
  151.6 3.1 multiply_reduce_fusion
  154.8 0.9 multiply_convert_fusion.1
  155.8 0.7 all-gather.11.cloned.1.call-update
  157.3 18.8 %all-gather.7.cloned.1.call-done = bf16[512,2048]{1,0:T(8,128)(2,1)} async-done(((bf16[128,2048]{1,0:T(8,128)(2,1)}), bf16[512,2048]{1,0:T(8,128)(2,1)}) %all-gather.7.cloned.1.call-update) | async-done | bytes 2097168 | tf_op jit(solution)/shard_map/all_gather | solution.py:64
  176.1 127.0 %all-gather.11.cloned.1.call-done = bf16[2048,2048]{1,0:T(8,128)(2,1)} async-done(((bf16[2048,256]{1,0:T(8,128)(2,1)}), bf16[2048,2048]{1,0:T(8,128)(2,1)}) %all-gather.11.cloned.1.call-update) | async-done | bytes 8388624 | tf_op jit(solution)/shard_map/all_gather | solution.py:71
  303.1 124.7 %all-gather.9.cloned.1.call-done = bf16[2048,2048]{1,0:T(8,128)(2,1)} async-done(((bf16[256,2048]{1,0:T(8,128)(2,1)}), bf16[2048,2048]{1,0:T(8,128)(2,1)}) %all-gather.9.cloned.1.call-update) | async-done | bytes 8388624 | tf_op jit(solution)/shard_map/all_gather | solution.py:67
  427.8 16.5 %convolution_convert_fusion = bf16[512,2048]{1,0:T(8,128)(2,1)} fusion(bf16[2048,2048]{1,0:T(8,128)(2,1)} %all-gather.11.cloned.1.call-done, bf16[512,2048]{1,0:T(8,128)(2,1)} %all-gather.7.cloned.1.call-done, bf16[2048,2048]{1,0:T(8,128)(2,1)} %all-gather.9.cloned.1.call-done), kind=kOutput, calls=%fused_computation.30 | convolution fusion | flops 8594128896 | bytes 20971520 | tf_op jit(solution)/shard_map/dot_general | solution.py:72
  444.3 29.5 %reduce-scatter.2.cloned.1.call-done = bf16[128,2048]{1,0:T(8,128)(2,1)} async-done(((bf16[512,2048]{1,0:T(8,128)(2,1)}), bf16[128,2048]{1,0:T(8,128)(2,1)}) %reduce-scatter.2.cloned.1.call-update) | async-done | bytes 524304 | tf_op jit(solution)/shard_map/reduce_scatter | solution.py:73
  473.8 1.9 add_convert_fusion
  (35 shorter events, 3.7 us)
Async XLA Ops:
  6.5 78.7 %all-gather.5.cloned.1.call-start = ((), (), s32[]{:S(2)}) async-start(), calls=%async_computation.2 | async-start | bytes 4718592 | tf_op jit(solution)/shard_map/all_gather | solution.py:24
  8.4 167.7 %all-gather.7.cloned.1.call-start = ((), (), s32[]{:S(2)}) async-start(), calls=%async_computation.3 | async-start | bytes 2621440 | tf_op jit(solution)/shard_map/all_gather | solution.py:64
  43.0 52.0 %copy-start = (f32[512,2]{0,1:T(2,128)S(1)}, f32[512,2]{0,1:T(2,128)}, u32[]{:S(2)}) copy-start(f32[512,2]{0,1:T(2,128)} %param.14) | copy-start | bytes 12292
  141.6 13.2 %copy-start.1 = (f32[2048]{0:T(1024)S(1)}, f32[2048]{0:T(1024)}, u32[]{:S(2)}) copy-start(f32[2048]{0:T(1024)} %param.17) | copy-start | bytes 24580
  155.7 147.4 %all-gather.11.cloned.1.call-start = ((), (), s32[]{:S(2)}) async-start(), calls=%async_computation.5 | async-start | bytes 9437184 | tf_op jit(solution)/shard_map/all_gather | solution.py:71
  156.5 271.3 %all-gather.9.cloned.1.call-start = ((), (), s32[]{:S(2)}) async-start(), calls=%async_computation.4 | async-start | bytes 9437184 | tf_op jit(solution)/shard_map/all_gather | solution.py:67
  157.1 316.7 %reduce-scatter.2.cloned.1.call-start = ((), (), s32[]{:S(2)}) async-start(), calls=%async_computation.6 | async-start | bytes 2621440 | tf_op jit(solution)/shard_map/reduce_scatter | solution.py:73
Sparse Core Ops, SparseCore 0:
  9.5 75.7 all-gather.4
  155.9 20.1 all-gather.6
  178.1 124.9 all-gather.10
  305.1 122.6 all-gather.8
  444.4 29.3 reduce-scatter.1
